TPU v7x, 32 devices: a whole 2x2x4 slice. The times are simulated.
32 devices in a mesh: fs: 8 (over z, x), tp: 4 (over y, core).
Axes of the slice: x: 2, y: 2, z: 4, core: 2. Of those that a mesh axis runs over, the one named last changes fastest.
Arguments:
- tokens: bfloat16 [8192, 2048], P(('fs', 'tp')), may hold values from -130 to 130
- pool_weight: bfloat16 [4, 512, 512], P(None, 'fs'), may hold values from -0.25 to 0.25
- pool_scale: float32 [2048], replicated, may hold values from 0.5 to 1.5
- gain_mix: float32 [2048], replicated, may hold values from 0.1 to 1.9
- gain_mlp: float32 [2048], replicated, may hold values from 0.1 to 1.9
- w_up: bfloat16 [8192, 2048], P('tp', 'fs'), may hold values from -0.125 to 0.125
- w_down: bfloat16 [8192, 2048], P('tp', 'fs'), may hold values from -0.0625 to 0.0625
- gain_out: float32 [2048], P('tp'), may hold values from 0.1 to 1.9
Outputs:
- result: bfloat16 [8192, 2048], P('fs', 'tp')
All inputs are finite; a program needn't handle non-finite values.
Results may differ from a plain program's by a relative error of at most 0.013.
Values may be sent and summed in bfloat16 or wider, within the bound.
A program may use at most 64 MiB of HBM per device.

v0:
```python
import jax
import jax.numpy as jnp
from jax import lax
from jax.sharding import PartitionSpec as P

D = 2048
SEQ_LEN = 1024
EPS = 1e-06
WINDOWS = (2, 4, 8, 16)


def extended_2(x, sides, width):
    for axis, dim in sides:
        peers, length = (lax.axis_size(axis), x.shape[dim])
        up = [(i, (i + 1) % peers) for i in range(peers - 1)]
        down = [(j, i) for i, j in up]
        last = lax.slice_in_dim(x, length - width, length, axis=dim)
        first = lax.slice_in_dim(x, 0, width, axis=dim)
        before = lax.ppermute(last, axis, up)
        after = lax.ppermute(first, axis, down)
        x = jnp.concatenate([before, x, after], axis=dim)
    return x


def rms_scale(values, gain):
    return values * lax.rsqrt(jnp.mean(values * values, axis=-1, keepdims=True) + EPS) * gain


def local(tokens, pool_weight, pool_scale, gain_mix, gain_mlp, w_up, w_down, gain_out):
    rows = tokens.shape[0]
    width = tokens.shape[1]
    group = width // 4
    offset = lax.axis_index("tp") * rows
    inputs = tokens.astype(jnp.float32)
    normed = rms_scale(inputs, gain_mix).astype(jnp.bfloat16)
    extended = extended_2(normed, (("tp", 0),), 8).astype(jnp.float32)
    line = jnp.arange(rows + 16, dtype=jnp.int32)
    lower_open = offset % SEQ_LEN != 0
    upper_open = (offset + rows) % SEQ_LEN != 0
    keep = jnp.where(line < 8, lower_open, jnp.where(line >= rows + 8, upper_open, True))
    level = extended * keep.astype(jnp.float32)[:, None]
    position = (offset + jnp.arange(rows, dtype=jnp.int32)) % SEQ_LEN
    normed_f32 = normed.astype(jnp.float32)
    full_pool = lax.all_gather(pool_weight, "fs", axis=1, tiled=True)
    pieces = []
    for index, reach in enumerate(WINDOWS):
        half = reach // 2
        level = level[:-half] + level[half:]
        start = 8 - half
        window = level[start : start + rows, :group]
        lower = jnp.maximum(position - half, 0)
        upper = jnp.minimum(position + half, SEQ_LEN)
        counts = (upper - lower).astype(jnp.float32)[:, None]
        own = normed_f32[:, index * group : (index + 1) * group]
        pooled = (window / counts - own).astype(jnp.bfloat16)
        pieces.append(jnp.dot(pooled, full_pool[index], preferred_element_type=jnp.float32))
        level = level[:, group:]
    mixed = jnp.concatenate(pieces, axis=1) * pool_scale
    first_sum = (inputs + mixed).astype(jnp.bfloat16)
    inner = rms_scale(first_sum.astype(jnp.float32), gain_mlp).astype(jnp.bfloat16)
    all_inner = lax.all_gather(inner, "tp", axis=0, tiled=True)
    contract = (((1,), (1,)), ((), ()))
    pre = lax.dot_general(
        all_inner,
        lax.all_gather(w_up, "fs", axis=1, tiled=True),
        contract,
        preferred_element_type=jnp.float32,
    )
    hidden = jnp.square(jax.nn.relu(pre)).astype(jnp.bfloat16)
    partial_terms = jnp.dot(
        hidden, lax.all_gather(w_down, "fs", axis=1, tiled=True), preferred_element_type=jnp.float32
    )
    channel_out = lax.psum_scatter(
        partial_terms.astype(jnp.bfloat16), "tp", scatter_dimension=1, tiled=True
    ).astype(jnp.float32)
    first_columns = lax.all_to_all(first_sum, "tp", split_axis=1, concat_axis=0, tiled=True)
    second_sum = first_columns.astype(jnp.float32) + channel_out
    squares = lax.psum(jnp.sum(second_sum * second_sum, axis=1), "tp")
    scaled = second_sum * lax.rsqrt(squares / D + EPS)[:, None] * gain_out
    return scaled.astype(jnp.bfloat16)


def solution(mesh):
    return jax.shard_map(
        local,
        mesh=mesh,
        in_specs=(
            P(("fs", "tp"), None),
            P(None, "fs", None),
            P(),
            P(),
            P(),
            P("tp", "fs"),
            P("tp", "fs"),
            P("tp"),
        ),
        out_specs=P("fs", "tp"),
        check_vma=False,
    )
```

profile of v0, /device:TPU:0, one launch (start us, length us, event | category | flops | bytes accessed | tf_op | source)
XLA Modules:
  0.0 437.5 jit_solution(9384960922146906074)
XLA Ops:
  6.5 0.7 all-gather.5.cloned.1.call-update
  7.3 1.5 fusion.3
  8.8 2.9 fusion.30
  11.7 2.4 collective-permute-start
  14.1 1.3 collective-permute-start.1
  15.5 3.8 collective-permute-done.1
  20.1 1.2 copy-done.1
  21.4 1.1 fusion.32
  22.6 38.8 %all-gather.5.cloned.1.call-done = bf16[4,512,512]{2,1,0:T(8,128)(2,1)} async-done(((bf16[4,64,512]{2,1,0:T(8,128)(2,1)}), bf16[4,512,512]{2,1,0:T(8,128)(2,1)}) %all-gather.5.cloned.1.call-update) | async-done | bytes 2097168 | tf_op jit(solution)/shard_map/all_gather | solution.py:44
  61.3 1.7 fusion.14
  63.2 1.7 fusion.12
  65.4 0.6 copy-done.4
  66.7 0.5 fusion
  67.4 1.3 fusion.2
  68.7 0.7 all-gather.9.cloned.1.call-update
  70.0 31.8 %all-gather.7.cloned.1.call-done = bf16[1024,2048]{1,0:T(8,128)(2,1)} async-done(((bf16[256,2048]{1,0:T(8,128)(2,1)}), bf16[1024,2048]{1,0:T(8,128)(2,1)}) %all-gather.7.cloned.1.call-update) | async-done | bytes 4194320 | tf_op jit(solution)/shard_map/all_gather | solution.py:61
  101.8 127.0 %all-gather.9.cloned.1.call-done = bf16[2048,2048]{1,0:T(8,128)(2,1)} async-done(((bf16[2048,256]{1,0:T(8,128)(2,1)}), bf16[2048,2048]{1,0:T(8,128)(2,1)}) %all-gather.9.cloned.1.call-update) | async-done | bytes 8388624 | tf_op jit(solution)/shard_map/all_gather | solution.py:65
  228.8 125.0 %all-gather.11.cloned.1.call-done = bf16[2048,2048]{1,0:T(8,128)(2,1)} async-done(((bf16[2048,256]{1,0:T(8,128)(2,1)}), bf16[2048,2048]{1,0:T(8,128)(2,1)}) %all-gather.11.cloned.1.call-update) | async-done | bytes 8388624 | tf_op jit(solution)/shard_map/all_gather | solution.py:71
  353.9 25.5 %convolution_convert_fusion = bf16[1024,2048]{1,0:T(8,128)(2,1)} fusion(bf16[2048,2048]{1,0:T(8,128)(2,1)} %all-gather.11.cloned.1.call-done, bf16[1024,2048]{1,0:T(8,128)(2,1)} %all-gather.7.cloned.1.call-done, bf16[2048,2048]{1,0:T(8,128)(2,1)} %all-gather.9.cloned.1.call-done), kind=kOutput, calls=%fused_computation.1 | convolution fusion | flops 17188257792 | bytes 25165824 | tf_op jit(solution)/shard_map/dot_general | solution.py:70
  379.5 17.0 %all_to_all.13 = bf16[256,4,512]{2,0,1:T(8,128)(2,1)S(1)} all-to-all(bf16[256,4,512]{2,0,1:T(8,128)(2,1)S(1)} %bitcast.28), channel_id=1, replica_groups=mesh['fs'=8,'tp'=4] {'tp'}, dimensions={1} | all-to-all | bytes 2097152 | tf_op jit(solution)/shard_map/all_to_all | solution.py:76
  396.5 25.6 %reduce-scatter.2.cloned.1.call-done = bf16[1024,512]{1,0:T(8,128)(2,1)} async-done(((bf16[1024,2048]{1,0:T(8,128)(2,1)}), bf16[1024,512]{1,0:T(8,128)(2,1)}) %reduce-scatter.2.cloned.1.call-update) | async-done | bytes 1048592 | tf_op jit(solution)/shard_map/reduce_scatter | solution.py:73
  422.1 1.7 multiply_reduce_fusion
  423.8 5.8 %psum.7 = f32[1024]{0:T(1024)S(1)} all-reduce(f32[1024]{0:T(1024)S(1)} %multiply_reduce_fusion), channel_id=1, replica_groups=mesh['fs'=8,'tp'=4] {'tp'}, use_global_device_ids=true, to_apply=%region_4.5 | all-reduce | flops 1024 | bytes 8192 | tf_op jit(solution)/shard_map/psum | solution.py:78
  429.6 1.4 multiply_convert_fusion.1
  (41 shorter events, 3.2 us)
Async XLA Ops:
  6.5 54.8 %all-gather.5.cloned.1.call-start = ((), (), s32[]{:S(2)}) async-start(), calls=%async_computation.2 | async-start | bytes 2359296 | tf_op jit(solution)/shard_map/all_gather | solution.py:44
  7.3 94.6 %all-gather.7.cloned.1.call-start = ((), (), s32[]{:S(2)}) async-start(), calls=%async_computation.3 | async-start | bytes 5242880 | tf_op jit(solution)/shard_map/all_gather | solution.py:61
  11.7 3.8 collective-permute-start
  14.1 5.2 %collective-permute-start.1 = (bf16[8,2048]{1,0:T(8,128)(2,1)S(1)}, bf16[8,2048]{1,0:T(8,128)(2,1)S(1)}, u32[]{:S(2)}, u32[]{:S(2)}) collective-permute-start(bf16[8,2048]{1,0:T(8,128)(2,1)S(1)} %get-tuple-element.12), channel_id=1, source_target_pairs={{1,0},{2,1},{3,2},{5,4},{6,5},{7,6},{9,8},{10,9},{11,10},{13,12},{... | collective-permute-start | bytes 98312 | tf_op jit(solution)/shard_map/ppermute | solution.py:20
  20.1 1.2 copy-start.1
  61.3 1.9 copy-start.3
  63.0 2.0 copy-start.9
  64.9 1.1 copy-start.4
  64.9 1.2 copy-start.5
  65.4 1.3 copy-start
  65.4 1.3 copy-start.6
  66.7 0.7 copy-start.7
  68.7 160.2 %all-gather.9.cloned.1.call-start = ((), (), s32[]{:S(2)}) async-start(), calls=%async_computation.4 | async-start | bytes 9437184 | tf_op jit(solution)/shard_map/all_gather | solution.py:65
  69.4 284.5 %all-gather.11.cloned.1.call-start = ((), (), s32[]{:S(2)}) async-start(), calls=%async_computation.5 | async-start | bytes 9437184 | tf_op jit(solution)/shard_map/all_gather | solution.py:71
  70.0 352.1 %reduce-scatter.2.cloned.1.call-start = ((), (), s32[]{:S(2)}) async-start(), calls=%async_computation.6 | async-start | bytes 5242880 | tf_op jit(solution)/shard_map/reduce_scatter | solution.py:73
  379.5 50.1 %copy-start.8 = (f32[512]{0:T(512)S(1)}, f32[512]{0:T(512)}, u32[]{:S(2)}) copy-start(f32[512]{0:T(512)} %param.15) | copy-start | bytes 6148
  422.1 7.5 %copy-start.2 = (bf16[1024,512]{1,0:T(8,128)(2,1)S(1)}, bf16[1024,512]{1,0:T(8,128)(2,1)}, u32[]{:S(2)}) copy-start(bf16[1024,512]{1,0:T(8,128)(2,1)} %reduce-scatter.2.cloned.1.call-done) | copy-start | bytes 3145732
Sparse Core Ops, SparseCore 0:
  9.5 51.7 all-gather.4
  68.8 32.9 all-gather.6
  103.9 124.9 all-gather.8
  230.7 123.1 all-gather.10
  379.5 42.5 reduce-scatter.1
where the time goes:
time: 438 us
  waiting for transfers between devices  354 us (81%)
  matrix products  29.5 us (7%)
  blocking collectives  22.8 us (5%)
  between operations  13.3 us (3%)
  other arithmetic  10.2 us (2%)
    all_gather x1, waiting for transfers between devices, local(): lax.all_gather(w_up, 'fs', axis=1, tiled=True)  127 us
    all_gather x1, waiting for transfers between devices, local(): lax.all_gather(w_down, 'fs', axis=1, tiled=True)  125 us
    all_gather x1, waiting for transfers between devices, local(): full_pool = lax.all_gather(pool_weight, 'fs', axis=1, tiled=True)  38.8 us
    all_gather x1, waiting for transfers between devices, local(): all_inner = lax.all_gather(inner, 'tp', axis=0, tiled=True)  31.8 us
    reduce_scatter x1, waiting for transfers between devices, local(): lax.psum_scatter(partial_terms.astype(jnp.bfloat16), 'tp', scatter_dimens...  25.6 us
    dot_general x1, matrix products, local(): jnp.dot(hidden, lax.all_gather(w_down, 'fs', axis=1, tiled=True), preferr...  25.5 us
    all_to_all x1, blocking collectives, local(): lax.all_to_all(first_sum, 'tp', split_axis=1, concat_axis=0, tiled=True)  17 us
  transfers between devices with their start and end apart: 7, of which 6 were waited for; matrix products, arithmetic and copies ran while one was open for 1% of the time, Pallas kernels for 0%

commit v1 on v0

--- a/solution.py
+++ b/solution.py
@@ -41,7 +41,12 @@
     level = extended * keep.astype(jnp.float32)[:, None]
     position = (offset + jnp.arange(rows, dtype=jnp.int32)) % SEQ_LEN
     normed_f32 = normed.astype(jnp.float32)
-    full_pool = lax.all_gather(pool_weight, "fs", axis=1, tiled=True)
+    ring = [pool_weight]
+    for hop in range(7):
+        ring.append(lax.ppermute(ring[-1], "fs", [(dev, (dev + 1) % 8) for dev in range(8)]))
+    full_pool = jnp.roll(
+        jnp.concatenate(ring[::-1], axis=1), (lax.axis_index("fs") + 1) * ring[0].shape[1], axis=1
+    )
     pieces = []
     for index, reach in enumerate(WINDOWS):
         half = reach // 2

time: 438 us -> 451 us (1.030)
  waiting for transfers between devices: 354 us -> 368 us
    ppermute x0 -> x7, waiting for transfers between devices: none -> 58.6 us  [local(): lax.ppermute(ring[-1], 'fs', [(dev, (dev + 1) % 8) for dev in range(8)])]
    all_gather x1 -> x0, waiting for transfers between devices: 38.8 us -> none  [local(): full_pool = lax.all_gather(pool_weight, 'fs', axis=1, tiled=True)]
  transfers between devices with their start and end apart: 7 -> 13, of which waited for: 6 -> 11; matrix products, arithmetic and copies ran while one was open for 1% -> 1% of each run, Pallas kernels for 0% -> 0%
where the time goes in v1:
time: 451 us; the launch traced here: 450 us
  waiting for transfers between devices  368 us (82%)
  matrix products  26.9 us (6%)
  blocking collectives  22.8 us (5%)
  between operations  13.4 us (3%)
  other arithmetic  9.56 us (2%)
  starting transfers between devices  5.85 us (1%)
    all_gather x1, waiting for transfers between devices, local(): lax.all_gather(w_up, 'fs', axis=1, tiled=True)  127 us
    all_gather x1, waiting for transfers between devices, local(): lax.all_gather(w_down, 'fs', axis=1, tiled=True)  125 us
    ppermute x7, waiting for transfers between devices, local(): lax.ppermute(ring[-1], 'fs', [(dev, (dev + 1) % 8) for dev in range(8)])  58.6 us
    all_gather x1, waiting for transfers between devices, local(): all_inner = lax.all_gather(inner, 'tp', axis=0, tiled=True)  30.2 us
    reduce_scatter x1, waiting for transfers between devices, local(): lax.psum_scatter(partial_terms.astype(jnp.bfloat16), 'tp', scatter_dimens...  25.6 us
    dot_general x1, matrix products, local(): jnp.dot(hidden, lax.all_gather(w_down, 'fs', axis=1, tiled=True), preferr...  25.4 us
    all_to_all x1, blocking collectives, local(): lax.all_to_all(first_sum, 'tp', split_axis=1, concat_axis=0, tiled=True)  17 us
  transfers between devices with their start and end apart: 13, of which 11 were waited for; matrix products, arithmetic and copies ran while one was open for 1% of the time, Pallas kernels for 0%

profile of v1, /device:TPU:0, one launch (start us, length us, event | category | flops | bytes accessed | tf_op | source)
XLA Modules:
  0.0 450.3 jit_solution(7362654987262233278)
XLA Ops:
  6.5 3.0 collective-permute-start.2
  9.5 1.5 fusion.3
  11.0 1.6 fusion.34
  12.6 1.5 collective-permute-start
  14.1 1.3 collective-permute-start.1
  15.4 3.7 collective-permute-done.2
  19.7 9.6 %collective-permute-done.3 = bf16[4,64,512]{2,1,0:T(8,128)(2,1)} collective-permute-done((bf16[4,64,512]{2,1,0:T(8,128)(2,1)S(1)}, bf16[4,64,512]{2,1,0:T(8,128)(2,1)}, u32[]{:S(2)}, u32[]{:S(2)}) %collective-permute-start.3) | collective-permute-done | bytes 262176 | tf_op jit(solution)/shard_map/ppermute | solution.py:46
  29.6 9.3 %collective-permute-done.4 = bf16[4,64,512]{2,1,0:T(8,128)(2,1)S(1)} collective-permute-done((bf16[4,64,512]{2,1,0:T(8,128)(2,1)}, bf16[4,64,512]{2,1,0:T(8,128)(2,1)S(1)}, u32[]{:S(2)}, u32[]{:S(2)}) %collective-permute-start.4) | collective-permute-done | bytes 262176 | tf_op jit(solution)/shard_map/ppermute | solution.py:46
  39.2 8.7 %collective-permute-done.5 = bf16[4,64,512]{2,1,0:T(8,128)(2,1)S(1)} collective-permute-done((bf16[4,64,512]{2,1,0:T(8,128)(2,1)S(1)}, bf16[4,64,512]{2,1,0:T(8,128)(2,1)S(1)}, u32[]{:S(2)}, u32[]{:S(2)}) %collective-permute-start.5) | collective-permute-done | bytes 262176 | tf_op jit(solution)/shard_map/ppermute | solution.py:46
  48.2 8.8 %collective-permute-done.6 = bf16[4,64,512]{2,1,0:T(8,128)(2,1)S(1)} collective-permute-done((bf16[4,64,512]{2,1,0:T(8,128)(2,1)S(1)}, bf16[4,64,512]{2,1,0:T(8,128)(2,1)S(1)}, u32[]{:S(2)}, u32[]{:S(2)}) %collective-permute-start.6) | collective-permute-done | bytes 262176 | tf_op jit(solution)/shard_map/ppermute | solution.py:46
  57.2 9.5 %collective-permute-done.7 = bf16[4,64,512]{2,1,0:T(8,128)(2,1)S(1)} collective-permute-done((bf16[4,64,512]{2,1,0:T(8,128)(2,1)S(1)}, bf16[4,64,512]{2,1,0:T(8,128)(2,1)S(1)}, u32[]{:S(2)}, u32[]{:S(2)}) %collective-permute-start.7) | collective-permute-done | bytes 262176 | tf_op jit(solution)/shard_map/ppermute | solution.py:46
  66.8 8.9 %collective-permute-done.8 = bf16[4,64,512]{2,1,0:T(8,128)(2,1)S(1)} collective-permute-done((bf16[4,64,512]{2,1,0:T(8,128)(2,1)S(1)}, bf16[4,64,512]{2,1,0:T(8,128)(2,1)S(1)}, u32[]{:S(2)}, u32[]{:S(2)}) %collective-permute-start.8) | collective-permute-done | bytes 262176 | tf_op jit(solution)/shard_map/ppermute | solution.py:46
  75.9 1.0 constant_dynamic-update-slice_fusion.10
  77.0 1.0 constant_dynamic-update-slice_fusion.2
  81.4 1.3 fusion.2
  84.3 30.2 %all-gather.4.cloned.1.call-done = bf16[1024,2048]{1,0:T(8,128)(2,1)} async-done(((bf16[256,2048]{1,0:T(8,128)(2,1)}), bf16[1024,2048]{1,0:T(8,128)(2,1)}) %all-gather.4.cloned.1.call-update) | async-done | bytes 4194320 | tf_op jit(solution)/shard_map/all_gather | solution.py:66
  114.4 127.0 %all-gather.6.cloned.1.call-done = bf16[2048,2048]{1,0:T(8,128)(2,1)} async-done(((bf16[2048,256]{1,0:T(8,128)(2,1)}), bf16[2048,2048]{1,0:T(8,128)(2,1)}) %all-gather.6.cloned.1.call-update) | async-done | bytes 8388624 | tf_op jit(solution)/shard_map/all_gather | solution.py:70
  241.4 125.2 %all-gather.8.cloned.1.call-done = bf16[2048,2048]{1,0:T(8,128)(2,1)} async-done(((bf16[2048,256]{1,0:T(8,128)(2,1)}), bf16[2048,2048]{1,0:T(8,128)(2,1)}) %all-gather.8.cloned.1.call-update) | async-done | bytes 8388624 | tf_op jit(solution)/shard_map/all_gather | solution.py:76
  366.6 25.4 %convolution_convert_fusion = bf16[1024,2048]{1,0:T(8,128)(2,1)} fusion(bf16[2048,2048]{1,0:T(8,128)(2,1)} %all-gather.8.cloned.1.call-done, bf16[1024,2048]{1,0:T(8,128)(2,1)} %all-gather.4.cloned.1.call-done, bf16[2048,2048]{1,0:T(8,128)(2,1)} %all-gather.6.cloned.1.call-done), kind=kOutput, calls=%fused_computation.1 | convolution fusion | flops 17188257792 | bytes 25165824 | tf_op jit(solution)/shard_map/dot_general | solution.py:75
  392.2 17.0 %all_to_all.13 = bf16[256,4,512]{2,0,1:T(8,128)(2,1)S(1)} all-to-all(bf16[256,4,512]{2,0,1:T(8,128)(2,1)S(1)} %bitcast.28), channel_id=1, replica_groups=mesh['fs'=8,'tp'=4] {'tp'}, dimensions={1} | all-to-all | bytes 2097152 | tf_op jit(solution)/shard_map/all_to_all | solution.py:81
  409.2 25.6 %reduce-scatter.2.cloned.1.call-done = bf16[1024,512]{1,0:T(8,128)(2,1)} async-done(((bf16[1024,2048]{1,0:T(8,128)(2,1)}), bf16[1024,512]{1,0:T(8,128)(2,1)}) %reduce-scatter.2.cloned.1.call-update) | async-done | bytes 1048592 | tf_op jit(solution)/shard_map/reduce_scatter | solution.py:78
  434.9 1.7 multiply_reduce_fusion
  436.6 5.8 %psum.7 = f32[1024]{0:T(1024)S(1)} all-reduce(f32[1024]{0:T(1024)S(1)} %multiply_reduce_fusion), channel_id=1, replica_groups=mesh['fs'=8,'tp'=4] {'tp'}, use_global_device_ids=true, to_apply=%region_4.5 | all-reduce | flops 1024 | bytes 8192 | tf_op jit(solution)/shard_map/psum | solution.py:83
  442.4 1.4 multiply_convert_fusion.1
  (62 shorter events, 6.9 us)
Async XLA Ops:
  6.5 107.9 %all-gather.4.cloned.1.call-start = ((), (), s32[]{:S(2)}) async-start(), calls=%async_computation.2 | async-start | bytes 5242880 | tf_op jit(solution)/shard_map/all_gather | solution.py:66
  6.5 12.5 %collective-permute-start.2 = (bf16[4,64,512]{2,1,0:T(8,128)(2,1)}, bf16[4,64,512]{2,1,0:T(8,128)(2,1)S(1)}, u32[]{:S(2)}, u32[]{:S(2)}) collective-permute-start(bf16[4,64,512]{2,1,0:T(8,128)(2,1)} %param.9), channel_id=1, source_target_pairs={{0,4},{4,8},{8,12},{12,16},{16,20},{20,24},{24,28},{28,0},{1,5},{5... | collective-permute-start | bytes 786440 | tf_op jit(solution)/shard_map/ppermute | solution.py:46
  12.6 16.7 %collective-permute-start = (bf16[8,2048]{1,0:T(8,128)(2,1)S(1)}, bf16[8,2048]{1,0:T(8,128)(2,1)S(1)}, u32[]{:S(2)}, u32[]{:S(2)}) collective-permute-start(bf16[8,2048]{1,0:T(8,128)(2,1)S(1)} %get-tuple-element.11), channel_id=1, source_target_pairs={{0,1},{1,2},{2,3},{4,5},{5,6},{6,7},{8,9},{9,10},{10,11},{12,13},{... | collective-permute-start | bytes 98312 | tf_op jit(solution)/shard_map/ppermute | solution.py:19
  14.1 15.3 %collective-permute-start.1 = (bf16[8,2048]{1,0:T(8,128)(2,1)S(1)}, bf16[8,2048]{1,0:T(8,128)(2,1)S(1)}, u32[]{:S(2)}, u32[]{:S(2)}) collective-permute-start(bf16[8,2048]{1,0:T(8,128)(2,1)S(1)} %get-tuple-element.12), channel_id=1, source_target_pairs={{1,0},{2,1},{3,2},{5,4},{6,5},{7,6},{9,8},{10,9},{11,10},{13,12},{... | collective-permute-start | bytes 98312 | tf_op jit(solution)/shard_map/ppermute | solution.py:20
  19.1 10.3 %collective-permute-start.3 = (bf16[4,64,512]{2,1,0:T(8,128)(2,1)S(1)}, bf16[4,64,512]{2,1,0:T(8,128)(2,1)}, u32[]{:S(2)}, u32[]{:S(2)}) collective-permute-start(bf16[4,64,512]{2,1,0:T(8,128)(2,1)S(1)} %collective-permute-done.2), channel_id=1, source_target_pairs={{0,4},{4,8},{8,12},{12,16},{16,20},{20,24},{24,28},{28,0},{1,5},{5... | collective-permute-start | bytes 786440 | tf_op jit(solution)/shard_map/ppermute | solution.py:46
  29.3 9.5 %collective-permute-start.4 = (bf16[4,64,512]{2,1,0:T(8,128)(2,1)}, bf16[4,64,512]{2,1,0:T(8,128)(2,1)S(1)}, u32[]{:S(2)}, u32[]{:S(2)}) collective-permute-start(bf16[4,64,512]{2,1,0:T(8,128)(2,1)} %collective-permute-done.3), channel_id=1, source_target_pairs={{0,4},{4,8},{8,12},{12,16},{16,20},{20,24},{24,28},{28,0},{1,5},{5... | collective-permute-start | bytes 786440 | tf_op jit(solution)/shard_map/ppermute | solution.py:46
  38.9 9.1 %collective-permute-start.5 = (bf16[4,64,512]{2,1,0:T(8,128)(2,1)S(1)}, bf16[4,64,512]{2,1,0:T(8,128)(2,1)S(1)}, u32[]{:S(2)}, u32[]{:S(2)}) collective-permute-start(bf16[4,64,512]{2,1,0:T(8,128)(2,1)S(1)} %collective-permute-done.4), channel_id=1, source_target_pairs={{0,4},{4,8},{8,12},{12,16},{16,20},{20,24},{24,28},{28,0},{1,5},{5... | collective-permute-start | bytes 786440 | tf_op jit(solution)/shard_map/ppermute | solution.py:46
  47.9 9.1 %collective-permute-start.6 = (bf16[4,64,512]{2,1,0:T(8,128)(2,1)S(1)}, bf16[4,64,512]{2,1,0:T(8,128)(2,1)S(1)}, u32[]{:S(2)}, u32[]{:S(2)}) collective-permute-start(bf16[4,64,512]{2,1,0:T(8,128)(2,1)S(1)} %collective-permute-done.5), channel_id=1, source_target_pairs={{0,4},{4,8},{8,12},{12,16},{16,20},{20,24},{24,28},{28,0},{1,5},{5... | collective-permute-start | bytes 786440 | tf_op jit(solution)/shard_map/ppermute | solution.py:46
  57.0 9.7 %collective-permute-start.7 = (bf16[4,64,512]{2,1,0:T(8,128)(2,1)S(1)}, bf16[4,64,512]{2,1,0:T(8,128)(2,1)S(1)}, u32[]{:S(2)}, u32[]{:S(2)}) collective-permute-start(bf16[4,64,512]{2,1,0:T(8,128)(2,1)S(1)} %collective-permute-done.6), channel_id=1, source_target_pairs={{0,4},{4,8},{8,12},{12,16},{16,20},{20,24},{24,28},{28,0},{1,5},{5... | collective-permute-start | bytes 786440 | tf_op jit(solution)/shard_map/ppermute | solution.py:46
  66.7 9.1 %collective-permute-start.8 = (bf16[4,64,512]{2,1,0:T(8,128)(2,1)S(1)}, bf16[4,64,512]{2,1,0:T(8,128)(2,1)S(1)}, u32[]{:S(2)}, u32[]{:S(2)}) collective-permute-start(bf16[4,64,512]{2,1,0:T(8,128)(2,1)S(1)} %collective-permute-done.7), channel_id=1, source_target_pairs={{0,4},{4,8},{8,12},{12,16},{16,20},{20,24},{24,28},{28,0},{1,5},{5... | collective-permute-start | bytes 786440 | tf_op jit(solution)/shard_map/ppermute | solution.py:46
  66.8 10.1 %copy-start.2 = (bf16[4,64,512]{2,1,0:T(8,128)(2,1)S(1)}, bf16[4,64,512]{2,1,0:T(8,128)(2,1)}, u32[]{:S(2)}) copy-start(bf16[4,64,512]{2,1,0:T(8,128)(2,1)} %param.9) | copy-start | bytes 786436
  78.4 0.7 copy-start.6
  79.5 1.2 copy-start
  79.5 1.2 copy-start.3
  80.7 0.7 copy-start.4
  82.7 158.7 %all-gather.6.cloned.1.call-start = ((), (), s32[]{:S(2)}) async-start(), calls=%async_computation.3 | async-start | bytes 9437184 | tf_op jit(solution)/shard_map/all_gather | solution.py:70
  83.5 283.2 %all-gather.8.cloned.1.call-start = ((), (), s32[]{:S(2)}) async-start(), calls=%async_computation.4 | async-start | bytes 9437184 | tf_op jit(solution)/shard_map/all_gather | solution.py:76
  84.2 350.7 %reduce-scatter.2.cloned.1.call-start = ((), (), s32[]{:S(2)}) async-start(), calls=%async_computation.5 | async-start | bytes 5242880 | tf_op jit(solution)/shard_map/reduce_scatter | solution.py:78
  392.2 50.2 %copy-start.5 = (f32[512]{0:T(512)S(1)}, f32[512]{0:T(512)}, u32[]{:S(2)}) copy-start(f32[512]{0:T(512)} %param.15) | copy-start | bytes 6148
  434.9 7.5 %copy-start.1 = (bf16[1024,512]{1,0:T(8,128)(2,1)S(1)}, bf16[1024,512]{1,0:T(8,128)(2,1)}, u32[]{:S(2)}) copy-start(bf16[1024,512]{1,0:T(8,128)(2,1)} %reduce-scatter.2.cloned.1.call-done) | copy-start | bytes 3145732
Sparse Core Ops, SparseCore 0:
  82.8 31.5 all-gather.3
  116.5 124.9 all-gather.5
  243.5 123.1 all-gather.7
  392.2 42.5 reduce-scatter.1
